TPU v7x, 32 devices: a whole 2x2x4 slice. The times are simulated.
32 devices in a mesh: sp: 4 (over y, x), tp: 8 (over z, core).
Axes of the slice: x: 2, y: 2, z: 4, core: 2. Of those that a mesh axis runs over, the one named last changes fastest.
Arguments:
- stream: bfloat16 [8, 1536, 2048], P('tp', 'sp'), may hold values from -80 to 80
- norm_gain: float32 [2048], replicated, may hold values from 0.1 to 1.9
- w_lin: bfloat16 [1024, 2048], P('tp'), may hold values from -0.125 to 0.125
- w_gate: bfloat16 [1024, 2048], P('tp'), may hold values from -0.125 to 0.125
- conv_taps: bfloat16 [31, 1024], replicated, may hold values from -3 to 3
- conv_bias: float32 [1024], replicated, may hold values from -3 to 3
- ln_gain: float32 [1024], replicated, may hold values from 0.1 to 1.9
- ln_shift: float32 [1024], replicated, may hold values from -3 to 3
- w_proj: bfloat16 [1024, 2048], P('tp'), may hold values from -0.1875 to 0.1875
Outputs:
- result_stream: bfloat16 [8, 1536, 2048], P('tp', 'sp')
All inputs are finite; a program needn't handle non-finite values.
Results may differ from a plain program's by a relative error of at most 0.0024.
Values may be sent and summed in bfloat16 or wider, within the bound.
A program may use at most 64 MiB of HBM per device.

v0:
```python
import jax
import jax.numpy as jnp
from jax import lax
from jax.sharding import PartitionSpec as P

KW = 31


EPS = 1e-06


def passed_along(value, axis, steps):
    count = lax.axis_size(axis)
    leading, last = (max(0, -steps), min(count, count - steps))
    return lax.ppermute(value, axis, [(source, source + steps) for source in range(leading, last)])


def rms_rows(rows, gain):
    full = rows.astype(jnp.float32)
    scale = lax.rsqrt(jnp.mean(full * full, axis=1, keepdims=True) + EPS)
    return (full * scale * gain).astype(jnp.bfloat16)


def local(stream, norm_gain, w_lin, w_gate, conv_taps, conv_bias, ln_gain, ln_shift, w_proj):
    rows = stream.shape[1]
    reach = KW - 1
    current = stream[0]
    normed = rms_rows(current, norm_gain)
    paired = jnp.stack([w_lin, w_gate], axis=1)
    both = jnp.einsum(
        "td,nrd->trn",
        normed,
        lax.all_gather(paired, "tp", axis=0, tiled=True),
        preferred_element_type=jnp.float32,
    )
    linear = both[:, 0]
    gating = both[:, 1]
    mixed = (linear * jax.nn.sigmoid(gating)).astype(jnp.bfloat16)
    earlier_mixed = passed_along(mixed[rows - reach :], "sp", 1)
    padded = jnp.concatenate([earlier_mixed, mixed], axis=0).astype(jnp.float32)
    taps_full = conv_taps.astype(jnp.float32)
    conv = jnp.zeros((rows, mixed.shape[1]), jnp.float32)
    for tap in range(KW):
        conv = conv + taps_full[tap] * padded[tap : tap + rows]
    conv = conv + conv_bias
    mean = jnp.mean(conv, axis=1, keepdims=True)
    meansq = jnp.mean(conv * conv, axis=1, keepdims=True)
    var = meansq - mean * mean
    activated = jax.nn.silu((conv - mean) * lax.rsqrt(var + EPS) * ln_gain + ln_shift).astype(
        jnp.bfloat16
    )
    projected = jnp.dot(
        activated,
        lax.all_gather(w_proj, "tp", axis=0, tiled=True),
        preferred_element_type=jnp.float32,
    )
    return (current.astype(jnp.float32) + projected).astype(jnp.bfloat16)[None]


def solution(mesh):
    placed = (
        P("tp", "sp", None),
        P(),
        P("tp", None),
        P("tp", None),
        P(),
        P(),
        P(),
        P(),
        P("tp", None),
    )
    return jax.shard_map(
        local, mesh=mesh, in_specs=placed, out_specs=P("tp", "sp", None), check_vma=False
    )
```

profile of v0, /device:TPU:1, one launch (start us, length us, event | category | flops | bytes accessed | tf_op | source)
XLA Modules:
  0.0 153.0 jit_solution(13134745688078922933)
XLA Ops:
  6.5 0.0 all-gather.3.cloned.1.call-start
  6.5 0.0 copy-start
  6.5 2.4 %pad_maximum_fusion = bf16[128,2,2048]{2,0,1:T(8,128)(2,1)} fusion(bf16[128,1,2048]{2,0,1:T(8,128)(2,1)} %bitcast.54, bf16[128,1,2048]{2,0,1:T(8,128)(2,1)} %bitcast.55), kind=kLoop, calls=%fused_computation.83 | loop fusion | flops 524288 | bytes 2097152 | tf_op jit(solution)/shard_map/stack | solution.py:29
  8.9 0.0 copy-start.1
  8.9 0.0 copy-start.3
  8.9 0.0 all-gather.3.cloned.1.call-update
  9.0 0.0 all-gather.5.cloned.1.call-start
  9.0 0.7 all-gather.5.cloned.1.call-update
  9.7 0.0 copy-done
  9.7 0.4 fusion
  10.1 0.0 copy-done.1
  10.2 0.1 fusion.54
  10.2 83.4 %all-gather.3.cloned.1.call-done = bf16[1024,2,2048]{2,0,1:T(8,128)(2,1)} async-done(((bf16[128,2,2048]{2,0,1:T(8,128)(2,1)}), bf16[1024,2,2048]{2,0,1:T(8,128)(2,1)}) %all-gather.3.cloned.1.call-update) | async-done | bytes 8388624 | tf_op jit(solution)/shard_map/all_gather | solution.py:33
  93.6 0.0 copy-done.3
  93.6 5.9 %convolution_bitcast_fusion = f32[384,2,1024]{2,0,1:T(8,128)S(1)} fusion(bf16[1024,2,2048]{2,0,1:T(8,128)(2,1)} %all-gather.3.cloned.1.call-done, bf16[1,384,2048]{2,1,0:T(8,128)(2,1)S(1)} %copy-done, f32[2048]{0:T(1024)S(1)} %copy-done.3, f32[384]{0:T(512)S(1)} %add_rsqrt_fusion.1), kind=kOutput, calls=%fused_computation.8 | convolution fusion | flops 3224371200 | bytes 13116928 | tf_op jit(solution)/shard_map/td,nrd->trn/dot_general | solution.py:30
  99.5 0.4 fusion.45
  100.0 3.1 %collective-permute-start = (bf16[30,1024]{1,0:T(8,128)(2,1)S(1)}, bf16[30,1024]{1,0:T(8,128)(2,1)S(1)}, u32[]{:S(2)}, u32[]{:S(2)}) collective-permute-start(bf16[30,1024]{1,0:T(8,128)(2,1)S(1)} %slice_bitcast_fusion), channel_id=1, source_target_pairs={{0,8},{8,16},{16,24},{1,9},{9,17},{17,25},{2,10},{10,18},{18,26},{... | collective-permute-start | bytes 184328 | tf_op jit(solution)/shard_map/ppermute | solution.py:15
  103.1 0.4 fusion.58
  103.5 0.0 copy-start.2
  103.5 0.9 collective-permute-done
  104.4 0.2 maximum_convert_fusion
  104.6 0.0 copy-done.2
  104.6 0.0 copy-start.4
  104.6 0.0 copy-start.5
  104.7 7.5 %fusion.52 = (f32[384]{0:T(512)S(1)}, f32[384]{0:T(512)S(1)}, f32[384,1024]{1,0:T(8,128)S(1)}) fusion(f32[1024]{0:T(1024)S(1)} %copy-done.2, f32[414,1024]{1,0:T(8,128)S(1)} %maximum_convert_fusion, f32[1024]{0:T(1024)S(1)} %bitcast.67, f32[1024]{0:T(1024)S(1)} %bitcast.66, f32[1024]{0:T(1024)S(1)} %bitcast.65, f32[1024]{0:T(1024)S(1)} %bitcast.64, ...), kind=kLoop, calls=%fused_computation.95 | loop fusion | flops 25558272 | bytes 50465792 | tf_op jit(solution)/shard_map/reduce_sum | solution.py:46
  112.2 28.4 %all-gather.5.cloned.1.call-done = bf16[1024,2048]{1,0:T(8,128)(2,1)} async-done(((bf16[128,2048]{1,0:T(8,128)(2,1)}), bf16[1024,2048]{1,0:T(8,128)(2,1)}) %all-gather.5.cloned.1.call-update) | async-done | bytes 4194320 | tf_op jit(solution)/shard_map/all_gather | solution.py:54
  140.6 0.0 copy-done.4
  140.6 0.0 copy-done.5
  140.6 5.5 %fusion.4 = bf16[1,384,2048]{2,1,0:T(8,128)(2,1)} fusion(bf16[1024,2048]{1,0:T(8,128)(2,1)} %all-gather.5.cloned.1.call-done, bf16[1,384,2048]{2,1,0:T(8,128)(2,1)S(1)} %copy-done, f32[384,1024]{1,0:T(8,128)S(1)} %get-tuple-element.7, f32[1024]{0:T(1024)S(1)} %copy-done.4, f32[1024]{0:T(1024)S(1)} %copy-done.5, f32[384]{0:T(512)S(1)} %get-tuple-element.40, ...), kind=kOutput, calls=%fused_computation.7 | convolution fusion | flops 1616510976 | bytes 8924160 | tf_op jit(solution)/shard_map/dot_general | solution.py:52
  (4 shorter events, 0.1 us)
Async XLA Ops:
  6.5 87.1 %all-gather.3.cloned.1.call-start = ((), (), s32[]{:S(2)}) async-start(), calls=%async_computation | async-start | bytes 9437184 | tf_op jit(solution)/shard_map/all_gather | solution.py:33
  6.5 3.2 %copy-start = (bf16[1,384,2048]{2,1,0:T(8,128)(2,1)S(1)}, bf16[1,384,2048]{2,1,0:T(8,128)(2,1)}, u32[]{:S(2)}) copy-start(bf16[1,384,2048]{2,1,0:T(8,128)(2,1)} %param.9) | copy-start | bytes 4718596
  8.9 1.2 copy-start.1
  8.9 84.7 %copy-start.3 = (f32[2048]{0:T(1024)S(1)}, f32[2048]{0:T(1024)}, u32[]{:S(2)}) copy-start(f32[2048]{0:T(1024)} %param.10) | copy-start | bytes 24580
  9.0 131.6 %all-gather.5.cloned.1.call-start = ((), (), s32[]{:S(2)}) async-start(), calls=%async_computation.1 | async-start | bytes 4718592 | tf_op jit(solution)/shard_map/all_gather | solution.py:54
  100.0 4.4 %collective-permute-start = (bf16[30,1024]{1,0:T(8,128)(2,1)S(1)}, bf16[30,1024]{1,0:T(8,128)(2,1)S(1)}, u32[]{:S(2)}, u32[]{:S(2)}) collective-permute-start(bf16[30,1024]{1,0:T(8,128)(2,1)S(1)} %slice_bitcast_fusion), channel_id=1, source_target_pairs={{0,8},{8,16},{16,24},{1,9},{9,17},{17,25},{2,10},{10,18},{18,26},{... | collective-permute-start | bytes 184328 | tf_op jit(solution)/shard_map/ppermute | solution.py:15
  103.5 1.1 copy-start.2
  104.6 36.0 %copy-start.4 = (f32[1024]{0:T(1024)S(1)}, f32[1024]{0:T(1024)}, u32[]{:S(2)}) copy-start(f32[1024]{0:T(1024)} %param.16) | copy-start | bytes 12292
  104.6 36.0 %copy-start.5 = (f32[1024]{0:T(1024)S(1)}, f32[1024]{0:T(1024)}, u32[]{:S(2)}) copy-start(f32[1024]{0:T(1024)} %param.15) | copy-start | bytes 12292
Sparse Core Ops, SparseCore 0:
  9.1 84.4 all-gather.2
  95.2 45.3 all-gather.4
where the time goes:
time: 153 us
  waiting for transfers between devices  113 us (74%)
  between operations  13.5 us (9%)
  other arithmetic  11.4 us (7%)
  matrix products  11.4 us (7%)
  starting transfers between devices  3.14 us (2%)
    all_gather x1, waiting for transfers between devices, local(): lax.all_gather(paired, 'tp', axis=0, tiled=True)  83.4 us
    all_gather x1, waiting for transfers between devices, local(): lax.all_gather(w_proj, 'tp', axis=0, tiled=True)  28.4 us
    reduce_sum x1, other arithmetic, local(): mean = jnp.mean(conv, axis=1, keepdims=True)  7.54 us
    dot_general x1, matrix products, local(): jnp.einsum('td,nrd->trn', normed, lax.all_gather(paired, 'tp', axis=0, ti...  5.89 us
    dot_general x1, matrix products, local(): jnp.dot(activated, lax.all_gather(w_proj, 'tp', axis=0, tiled=True), pref...  5.54 us
    ppermute x1, starting transfers between devices, passed_along(): lax.ppermute(value, axis, [(source, source + steps) for source in range(l...  3.1 us
  transfers between devices with their start and end apart: 3, of which 3 were waited for; matrix products, arithmetic and copies ran while one was open for 10% of the time, Pallas kernels for 0%

commit v1 on v0

v1 whole, which is shorter than its diff:
```python
import functools

import jax
import jax.numpy as jnp
from jax import lax
from jax.experimental import pallas as pl
from jax.experimental.pallas import tpu as pltpu
from jax.sharding import PartitionSpec as P

EPS = 1e-06
HALO = 32
F32 = jnp.float32
BF16 = jnp.bfloat16
MESH = pl.DeviceIdType.MESH


def kernel(
    nsp, nz, kw,
    x_ref, gain_ref, wl_ref, wg_ref, wp_ref, taps_ref, bias_ref, lng_ref, lnb_ref,
    out_ref,
    held, xh, normed, mix, conv, act, taps,
    local_sem, halo_sem, z_recv, x_recv, y_recv, d_recv, up_send, dn_send, x_send, y_send, d_send,
):
    rows, width = x_ref.shape
    block = held.shape[2]
    shard = block // 2
    lanes = min(128, block)
    strips = block // lanes
    quarter = width // 4
    half = quarter // 2
    p, tp = lax.axis_index("sp"), lax.axis_index("tp")
    z, c = tp // 2, tp % 2
    q = p % 4
    low, high = q % 2, q // 2
    beside = (p + 1 - 2 * low, tp)
    across = (p + 2 - 4 * high, tp)
    twin = (p, z * 2 + 1 - c)
    above = (p, tp + 2)
    below = (p, tp - 2)
    parity = (low + high) % 2
    has_up, has_dn = z < nz - 1, z > 0
    has_next, has_prev = p < nsp - 1, p > 0
    qx, qy, qd = q + 1 - 2 * low, q + 2 - 4 * high, 3 - q

    def cols(start, size):
        return pl.ds(pl.multiple_of(start, 128), size)

    def at(kind, src, core, start, size):
        return held.at[kind, src, pl.ds(pl.multiple_of(core * shard, 16), shard), cols(start, size)]

    def send(piece, ssem, rsem, target):
        return pltpu.make_async_remote_copy(
            src_ref=piece, dst_ref=piece, send_sem=ssem, recv_sem=rsem, device_id=target, device_id_type=MESH
        )

    def z_piece(kind, src, i):
        if kind < 2:
            return at(kind, src, c, q * quarter, quarter)
        return at(kind, src, c, (parity * 2 + i) * quarter, quarter)

    def z_copy(kind, src, i, up):
        return send(
            z_piece(kind, src, i), (up_send if up else dn_send).at[kind, src, i], z_recv.at[kind, src, i],
            above if up else below,
        )

    def z_pieces(kind):
        return 1 if kind < 2 else 2

    def x_copy(kind, src, i, incoming):
        if kind == 2:
            piece = at(2, src, c, ((1 - parity if incoming else parity) * 2) * quarter, quarter)
        elif i == 0:
            piece = at(kind, src, c, (qx if incoming else q) * quarter, quarter)
        else:
            piece = at(kind, src, c, (qd if incoming else qy) * quarter, half)
        return send(piece, x_send.at[kind, src, i], x_recv.at[kind, src, i], beside)

    def y_copy(kind, src, i, incoming):
        if kind == 2:
            piece = at(2, src, c, ((1 - parity if incoming else parity) * 2 + 1) * quarter, quarter)
        elif i == 0:
            piece = at(kind, src, c, (qy if incoming else q) * quarter, quarter)
        else:
            piece = at(kind, src, c, (qd if incoming else qx) * quarter + half, half)
        return send(piece, y_send.at[kind, src, i], y_recv.at[kind, src, i], across)

    def d_copy(kind, src, core):
        return send(at(kind, src, core, 0, width), d_send.at[kind, src], d_recv.at[kind, src], twin)

    def halo_copy():
        return pltpu.make_async_remote_copy(
            src_ref=x_ref.at[pl.ds(rows - HALO, HALO)], dst_ref=xh, send_sem=halo_sem.at[0],
            recv_sem=halo_sem.at[1], device_id=(p + 1, tp), device_id_type=MESH,
        )

    mine = [
        pltpu.make_async_copy(ref, at(kind, z, c, 0, width), local_sem.at[kind])
        for kind, ref in enumerate((wl_ref, wg_ref, wp_ref))
    ]
    for copy in mine:
        copy.start()

    barrier = pltpu.get_barrier_semaphore()
    for target in (beside, across, twin):
        pl.semaphore_signal(barrier, inc=1, device_id=target, device_id_type=MESH)
    for there, target in (
        (has_up, above), (has_dn, below), (has_next, (p + 1, tp)), (has_prev, (p - 1, tp)),
    ):
        @pl.when(there)
        def _():
            pl.semaphore_signal(barrier, inc=1, device_id=target, device_id_type=MESH)

    one = lambda there: jnp.where(there, 1, 0)
    pl.semaphore_wait(barrier, 3 + one(has_up) + one(has_dn) + one(has_next) + one(has_prev))

    def start_own(kind):
        for i in range(z_pieces(kind)):
            @pl.when(has_up)
            def _():
                z_copy(kind, z, i, True).start()

            @pl.when(has_dn)
            def _():
                z_copy(kind, z, i, False).start()

    mine[0].wait()
    start_own(0)
    mine[1].wait()
    start_own(1)
    mine[2].wait()

    @pl.when(has_next)
    def _():
        halo_copy().start()

    for kind in range(3):
        d_copy(kind, z, c).start()

    def each(t, body):
        for sign in (-1, 1):
            src = z + sign * t

            @pl.when((src >= 0) & (src < nz))
            def _():
                body(src, sign)

    def relay(kind):
        def body(src, sign):
            for i in range(z_pieces(kind)):
                z_copy(kind, src, i, True).wait_recv()
                if sign < 0:
                    @pl.when(has_up)
                    def _():
                        z_copy(kind, src, i, True).start()
                else:
                    @pl.when(has_dn)
                    def _():
                        z_copy(kind, src, i, False).start()
                if kind < 2 or i == 0:
                    x_copy(kind, src, 0, False).start()
                if kind < 2 or i == 1:
                    y_copy(kind, src, 0, False).start()

        return body

    def diagonal(kind):
        def body(src, sign):
            x_copy(kind, src, 0, True).wait_recv()
            y_copy(kind, src, 1, False).start()
            y_copy(kind, src, 0, True).wait_recv()
            x_copy(kind, src, 1, False).start()

        return body

    def finish(kind):
        def body(src, sign):
            for i in ((1,) if kind < 2 else (0,)):
                x_copy(kind, src, i, True).wait_recv()
                y_copy(kind, src, i, True).wait_recv()
            d_copy(kind, src, c).start()

        return body

    def norm_into(ref, base, count):
        @pl.loop(0, count // 16)
        def _(r):
            full = ref[pl.ds(pl.multiple_of(r * 16, 16), 16), :].astype(F32)
            scale = lax.rsqrt(jnp.mean(full * full, axis=1, keepdims=True) + EPS)
            normed[pl.ds(pl.multiple_of(base + r * 16, 16), 16), :] = (full * scale * gain_ref[...]).astype(BF16)

    norm_into(x_ref, HALO, rows)
    for i in range(nz):
        taps[i, 0:kw] = taps_ref[:, i * block:(i + 1) * block].astype(F32)
        taps[i, kw:kw + 1] = bias_ref[:, i * block:(i + 1) * block]

    @pl.when(has_prev)
    def _():
        halo_copy().wait_recv()

    @pl.when(jnp.logical_not(has_prev))
    def _():
        xh[...] = jnp.zeros_like(xh)

    norm_into(xh, 0, HALO)

    tile = 64
    lead = HALO - (kw - 1)
    nt = (((1,), (1,)), ((), ()))

    def compute(t):
        def body(side, carry):
            src = z + (2 * side - 1) * t

            valid = (src >= 0) & (src < nz) & ((t > 0) | (side == 0))

            @pl.when(valid)
            def _():
                d_copy(0, src, 1 - c).wait_recv()
                d_copy(1, src, 1 - c).wait_recv()
                linear = lax.dot_general(normed[...], held[0, src], nt, preferred_element_type=F32)
                gating = lax.dot_general(normed[...], held[1, src], nt, preferred_element_type=F32)
                mixed = (linear * jax.nn.sigmoid(gating)).astype(BF16).astype(F32)
                for s in range(strips):
                    mix[s, 0:HALO + rows] = mixed[:, s * lanes:(s + 1) * lanes]

                @pl.loop(0, rows // tile)
                def _(r):
                    base = pl.multiple_of(r * tile, tile)
                    for s in range(strips):
                        lane = slice(s * lanes, (s + 1) * lanes)
                        total = jnp.broadcast_to(taps[src, kw:kw + 1, lane], (tile, lanes))
                        for b in range(8):
                            slab = mix[s, pl.ds(base + b, tile + HALO), :]
                            for a in range(HALO // 8 + 1):
                                tap = 8 * a + b - lead
                                if 0 <= tap < kw:
                                    total = total + taps[src, tap:tap + 1, lane] * slab[8 * a:8 * a + tile]
                        conv[src, pl.ds(base, tile), lane] = total

            return carry

        lax.fori_loop(0, 2, body, 0)

    @pl.loop(1, nz)
    def _(t):
        each(t, relay(0))
        each(t, relay(1))

        @pl.when(t == nz - 1)
        def _():
            start_own(2)

        each(t, diagonal(0))
        compute(t - 1)
        each(t, diagonal(1))
        each(t, finish(0))
        each(t, finish(1))

    each(1, relay(2))
    compute(nz - 1)

    @pl.loop(2, nz - 1)
    def _(t):
        each(t, relay(2))

    channels = nz * block

    @pl.loop(0, rows // 16)
    def _(r):
        here = pl.ds(pl.multiple_of(r * 16, 16), 16)
        parts = [conv[i, here, :] for i in range(nz)]
        mean = sum(jnp.sum(v, axis=1, keepdims=True) for v in parts) / channels
        meansq = sum(jnp.sum(v * v, axis=1, keepdims=True) for v in parts) / channels
        scale = lax.rsqrt(meansq - mean * mean + EPS)
        for i, v in enumerate(parts):
            lane = slice(i * block, (i + 1) * block)
            u = (v - mean) * scale * lng_ref[:, lane] + lnb_ref[:, lane]
            act[i, here, :] = (u * jax.nn.sigmoid(u)).astype(BF16)

    if nz > 2:
        each(nz - 1, relay(2))

    @pl.loop(1, nz)
    def _(t):
        each(t, finish(2))

    @pl.loop(0, nz)
    def _(src):
        d_copy(2, src, 1 - c).wait_recv()

    @pl.loop(0, 4)
    def _(n):
        here = cols(n * quarter, quarter)
        total = x_ref[:, here].astype(F32)
        for i in range(nz):
            total = total + jnp.dot(act[i], held[2, i, :, here], preferred_element_type=F32)
        out_ref[:, here] = total.astype(BF16)

    @pl.when(has_next)
    def _():
        halo_copy().wait_send()

    for kind in range(3):
        @pl.loop(0, nz)
        def _(src):
            d_copy(kind, src, c).wait_send()

            @pl.when(src != z)
            def _():
                for i in range(2 if kind < 2 else 1):
                    x_copy(kind, src, i, False).wait_send()
                    y_copy(kind, src, i, False).wait_send()

            for i in range(z_pieces(kind)):
                @pl.when((src <= z) & has_up)
                def _():
                    z_copy(kind, src, i, True).wait_send()

                @pl.when((src >= z) & has_dn)
                def _():
                    z_copy(kind, src, i, False).wait_send()


def local(nsp, ntp, stream, norm_gain, w_lin, w_gate, conv_taps, conv_bias, ln_gain, ln_shift, w_proj):
    _, rows, width = stream.shape
    kw, channels = conv_taps.shape
    nz = ntp // 2
    block = channels // nz
    lanes = min(128, block)
    vmem = pl.BlockSpec(memory_space=pltpu.VMEM)
    anyw = pl.BlockSpec(memory_space=pl.ANY)
    dma = pltpu.SemaphoreType.DMA
    out = pl.pallas_call(
        functools.partial(kernel, nsp, nz, kw),
        out_shape=jax.ShapeDtypeStruct((rows, width), BF16),
        in_specs=[vmem, vmem, anyw, anyw, anyw, vmem, vmem, vmem, vmem],
        out_specs=vmem,
        scratch_shapes=[
            pltpu.VMEM((3, nz, block, width), BF16),
            pltpu.VMEM((HALO, width), BF16),
            pltpu.VMEM((HALO + rows, width), BF16),
            pltpu.VMEM((block // lanes, HALO + rows + 8, lanes), F32),
            pltpu.VMEM((nz, rows, block), F32),
            pltpu.VMEM((nz, rows, block), BF16),
            pltpu.VMEM((nz, kw + 1, block), F32),
            dma((3,)), dma((2,)),
            dma((3, nz, 2)), dma((3, nz, 2)), dma((3, nz, 2)), dma((3, nz)),
            dma((3, nz, 2)), dma((3, nz, 2)), dma((3, nz, 2)), dma((3, nz, 2)), dma((3, nz)),
        ],
        compiler_params=pltpu.CompilerParams(
            collective_id=0, has_side_effects=True, vmem_limit_bytes=56 * 1024 * 1024
        ),
    )(
        stream[0], norm_gain[None], w_lin, w_gate, w_proj, conv_taps,
        conv_bias[None], ln_gain[None], ln_shift[None],
    )
    return out[None]


def solution(mesh):
    placed = (
        P("tp", "sp", None), P(), P("tp", None), P("tp", None), P(), P(), P(), P(), P("tp", None),
    )
    return jax.shard_map(
        functools.partial(local, mesh.shape["sp"], mesh.shape["tp"]),
        mesh=mesh, in_specs=placed, out_specs=P("tp", "sp", None), check_vma=False,
    )
```

time: 153 us -> 71.6 us (0.47)
  waiting for transfers between devices: 113 us -> 0 us
  Pallas kernels: 0 us -> 68.7 us
  between operations: 13.5 us -> 0.01 us
  matrix products: 11.4 us -> 0 us
  other arithmetic: 11.4 us -> 0 us
  starting transfers between devices: 3.14 us -> 0 us
  local copies, waits for them, and re-layouts: 0.14 us -> 2.73 us
    all_gather x2 -> x0, waiting for transfers between devices: 112 us -> none  [the longest x1 83.4 us: local(): lax.all_gather(paired, 'tp', axis=0, tiled=True)]
    pallas_call x0 -> x1, Pallas kernels: none -> 68.7 us  [local(): pl.pallas_call(functools.partial(kernel, nsp, nz, kw), out_shape=jax.Shap...]
    dot_general x2 -> x0, matrix products: 11.4 us -> none  [the longest x1 5.89 us: local(): jnp.einsum('td,nrd->trn', normed, lax.all_gather(paired, 'tp', axis=0, ti...]
    reduce_sum x2 -> x0, other arithmetic: 7.92 us -> none  [the longest x1 7.54 us: local(): mean = jnp.mean(conv, axis=1, keepdims=True)]
    ppermute x1 -> x0, starting transfers between devices: 3.1 us -> none  [passed_along(): lax.ppermute(value, axis, [(source, source + steps) for source in range(l...]
    unnamed x12 -> x1, local copies, waits for them, and re-layouts: 0.03 us -> 2.73 us
    another operation x1 -> x0, other arithmetic: 2.38 us -> none  [local(): paired = jnp.stack([w_lin, w_gate], axis=1)]
  transfers between devices with their start and end apart: 3 -> 0, of which waited for: 3 -> 0; matrix products, arithmetic and copies ran while one was open for 10% -> 0% of each run, Pallas kernels for 0% -> 0%
where the time goes in v1:
time: 71.6 us; the launch traced here: 71.4 us
  Pallas kernels  68.7 us (96%)
  local copies, waits for them, and re-layouts  2.73 us (4%)
    pallas_call x1, Pallas kernels, local(): pl.pallas_call(functools.partial(kernel, nsp, nz, kw), out_shape=jax.Shap...  68.7 us
    unnamed x1, local copies, waits for them, and re-layouts  2.73 us

profile of v1, /device:TPU:1, one launch (start us, length us, event | category | flops | bytes accessed | tf_op | source)
XLA Modules:
  0.0 71.4 jit_solution(3951287834589688728)
XLA Ops:
  0.0 68.7 %shard_map.91 = bf16[384,2048]{1,0:T(8,128)(2,1)} custom-call(bf16[384,2048]{1,0:T(8,128)(2,1)} %bitcast.7, f32[1,2048]{1,0:T(1,128)} %bitcast.8, bf16[128,2048]{1,0:T(8,128)(2,1)} %wl_ref.1, bf16[128,2048]{1,0:T(8,128)(2,1)} %wg_ref.1, bf16[128,2048]{1,0:T(8,128)(2,1)} %wp_ref.1, bf16[31,1024]{1,0:T(8,128)(2,1)} %taps_ref.1, f32[1,1024]{1,0:T(1,128)} %bitcast.9, ...), custom_call_target="tpu_custom_call" | custom-call | tf_op jit(solution)/shard_map/pallas_call | solution.py:334
  68.7 2.7 %copy.11 = bf16[1,384,2048]{2,1,0:T(8,128)(2,1)} copy(bf16[1,384,2048]{2,1,0:T(8,128)(2,1)} %bitcast.6) | data formatting | bytes 3145728

commit v2 on v1

--- a/solution.py
+++ b/solution.py
@@ -16,10 +16,10 @@
 
 def kernel(
     nsp, nz, kw,
-    x_ref, gain_ref, wl_ref, wg_ref, wp_ref, taps_ref, bias_ref, lng_ref, lnb_ref,
-    out_ref,
-    held, xh, normed, mix, conv, act, taps,
-    local_sem, halo_sem, z_recv, x_recv, y_recv, d_recv, up_send, dn_send, x_send, y_send, d_send,
+    x_any, gain_ref, wl_ref, wg_ref, wp_ref, taps_ref, bias_ref, lng_ref, lnb_ref,
+    out_any,
+    x_ref, out_ref, held, xh, normed, mix, conv, act, taps,
+    local_sem, out_sem, halo_sem, z_recv, x_recv, y_recv, d_recv, up_send, dn_send, x_send, y_send, d_send, dp_recv, dp_send,
 ):
     rows, width = x_ref.shape
     block = held.shape[2]
@@ -53,8 +53,11 @@
             src_ref=piece, dst_ref=piece, send_sem=ssem, recv_sem=rsem, device_id=target, device_id_type=MESH
         )
 
+    def final(kind):
+        return isinstance(kind, int) and kind == 2
+
     def z_piece(kind, src, i):
-        if kind < 2:
+        if not final(kind):
             return at(kind, src, c, q * quarter, quarter)
         return at(kind, src, c, (parity * 2 + i) * quarter, quarter)
 
@@ -65,10 +68,10 @@
         )
 
     def z_pieces(kind):
-        return 1 if kind < 2 else 2
+        return 2 if final(kind) else 1
 
     def x_copy(kind, src, i, incoming):
-        if kind == 2:
+        if final(kind):
             piece = at(2, src, c, ((1 - parity if incoming else parity) * 2) * quarter, quarter)
         elif i == 0:
             piece = at(kind, src, c, (qx if incoming else q) * quarter, quarter)
@@ -77,7 +80,7 @@
         return send(piece, x_send.at[kind, src, i], x_recv.at[kind, src, i], beside)
 
     def y_copy(kind, src, i, incoming):
-        if kind == 2:
+        if final(kind):
             piece = at(2, src, c, ((1 - parity if incoming else parity) * 2 + 1) * quarter, quarter)
         elif i == 0:
             piece = at(kind, src, c, (qy if incoming else q) * quarter, quarter)
@@ -88,6 +91,15 @@
     def d_copy(kind, src, core):
         return send(at(kind, src, core, 0, width), d_send.at[kind, src], d_recv.at[kind, src], twin)
 
+    def d_piece(kind, src, start, size):
+        return send(at(kind, src, c, start, size), d_send.at[kind, src], d_recv.at[kind, src], twin)
+
+    def p_cols(slot):
+        return ((parity + slot // 2) % 2 * 2 + slot % 2) * quarter
+
+    def p_copy(src, slot, core):
+        return send(at(2, src, core, p_cols(slot), quarter), dp_send.at[src, slot], dp_recv.at[src, slot], twin)
+
     def halo_copy():
         return pltpu.make_async_remote_copy(
             src_ref=x_ref.at[pl.ds(rows - HALO, HALO)], dst_ref=xh, send_sem=halo_sem.at[0],
@@ -98,8 +110,11 @@
         pltpu.make_async_copy(ref, at(kind, z, c, 0, width), local_sem.at[kind])
         for kind, ref in enumerate((wl_ref, wg_ref, wp_ref))
     ]
-    for copy in mine:
-        copy.start()
+    stream_in = pltpu.make_async_copy(x_any, x_ref, local_sem.at[3])
+    mine[0].start()
+    stream_in.start()
+    mine[1].start()
+    mine[2].start()
 
     barrier = pltpu.get_barrier_semaphore()
     for target in (beside, across, twin):
@@ -128,14 +143,27 @@
     start_own(0)
     mine[1].wait()
     start_own(1)
+    stream_in.wait()
+
+    @pl.when(has_next)
+    def _():
+        halo_copy().start()
+
+    d_copy(0, z, c).start()
+    d_copy(1, z, c).start()
     mine[2].wait()
-
-    @pl.when(has_next)
-    def _():
-        halo_copy().start()
-
-    for kind in range(3):
-        d_copy(kind, z, c).start()
+    for slot in range(4):
+        p_copy(z, slot, c).start()
+
+    @pl.when(has_up & (z == 0))
+    def _():
+        for i in range(2):
+            z_copy(2, z, i, True).start()
+
+    @pl.when(has_dn & (z == nz - 1))
+    def _():
+        for i in range(2):
+            z_copy(2, z, i, False).start()
 
     def each(t, body):
         for sign in (-1, 1):
@@ -145,22 +173,42 @@
             def _():
                 body(src, sign)
 
+    def pass_on(kind, src, sign, i):
+        z_copy(kind, src, i, True).wait_recv()
+        if sign < 0:
+            @pl.when(has_up)
+            def _():
+                z_copy(kind, src, i, True).start()
+        else:
+            @pl.when(has_dn)
+            def _():
+                z_copy(kind, src, i, False).start()
+
     def relay(kind):
         def body(src, sign):
-            for i in range(z_pieces(kind)):
-                z_copy(kind, src, i, True).wait_recv()
-                if sign < 0:
-                    @pl.when(has_up)
-                    def _():
-                        z_copy(kind, src, i, True).start()
-                else:
-                    @pl.when(has_dn)
-                    def _():
-                        z_copy(kind, src, i, False).start()
-                if kind < 2 or i == 0:
-                    x_copy(kind, src, 0, False).start()
-                if kind < 2 or i == 1:
-                    y_copy(kind, src, 0, False).start()
+            pass_on(kind, src, sign, 0)
+            x_copy(kind, src, 0, False).start()
+            y_copy(kind, src, 0, False).start()
+            d_piece(kind, src, q * quarter, quarter).start()
+
+        return body
+
+    def onward(i):
+        def body(src, sign):
+            pass_on(2, src, sign, i)
+            p_copy(src, i, c).start()
+
+        return body
+
+    def sideways(i):
+        def body(src, sign):
+            @pl.when(i == 0)
+            def _():
+                x_copy(2, src, 0, False).start()
+
+            @pl.when(i == 1)
+            def _():
+                y_copy(2, src, 0, False).start()
 
         return body
 
@@ -168,19 +216,27 @@
         def body(src, sign):
             x_copy(kind, src, 0, True).wait_recv()
             y_copy(kind, src, 1, False).start()
+            d_piece(kind, src, qx * quarter, quarter).start()
             y_copy(kind, src, 0, True).wait_recv()
             x_copy(kind, src, 1, False).start()
+            d_piece(kind, src, qy * quarter, quarter).start()
 
         return body
 
     def finish(kind):
         def body(src, sign):
-            for i in ((1,) if kind < 2 else (0,)):
-                x_copy(kind, src, i, True).wait_recv()
-                y_copy(kind, src, i, True).wait_recv()
-            d_copy(kind, src, c).start()
+            x_copy(kind, src, 1, True).wait_recv()
+            d_piece(kind, src, qd * quarter, half).start()
+            y_copy(kind, src, 1, True).wait_recv()
+            d_piece(kind, src, qd * quarter + half, half).start()
 
         return body
+
+    def arrived(src, sign):
+        x_copy(2, src, 0, True).wait_recv()
+        p_copy(src, 2, c).start()
+        y_copy(2, src, 0, True).wait_recv()
+        p_copy(src, 3, c).start()
 
     def norm_into(ref, base, count):
         @pl.loop(0, count // 16)
@@ -208,61 +264,109 @@
     lead = HALO - (kw - 1)
     nt = (((1,), (1,)), ((), ()))
 
-    def compute(t):
-        def body(side, carry):
+    def on_planes(t, body):
+        def one_side(side, carry):
             src = z + (2 * side - 1) * t
-
             valid = (src >= 0) & (src < nz) & ((t > 0) | (side == 0))
 
             @pl.when(valid)
             def _():
-                d_copy(0, src, 1 - c).wait_recv()
-                d_copy(1, src, 1 - c).wait_recv()
-                linear = lax.dot_general(normed[...], held[0, src], nt, preferred_element_type=F32)
-                gating = lax.dot_general(normed[...], held[1, src], nt, preferred_element_type=F32)
-                mixed = (linear * jax.nn.sigmoid(gating)).astype(BF16).astype(F32)
+                body(side, src)
+
+            return carry
+
+        lax.fori_loop(0, 2, one_side, 0)
+
+    def gate(t):
+        def body(side, src):
+            d_copy(0, src, 1 - c).wait_recv()
+            d_copy(1, src, 1 - c).wait_recv()
+            linear = lax.dot_general(normed[...], held[0, src], nt, preferred_element_type=F32)
+            gating = lax.dot_general(normed[...], held[1, src], nt, preferred_element_type=F32)
+            mixed = (linear * jax.nn.sigmoid(gating)).astype(BF16).astype(F32)
+            for s in range(strips):
+                mix[side, s, 0:HALO + rows] = mixed[:, s * lanes:(s + 1) * lanes]
+
+        on_planes(t, body)
+
+    def convolve(t):
+        def body(side, src):
+            @pl.loop(0, rows // tile)
+            def _(r):
+                base = pl.multiple_of(r * tile, tile)
                 for s in range(strips):
-                    mix[s, 0:HALO + rows] = mixed[:, s * lanes:(s + 1) * lanes]
-
-                @pl.loop(0, rows // tile)
-                def _(r):
-                    base = pl.multiple_of(r * tile, tile)
-                    for s in range(strips):
-                        lane = slice(s * lanes, (s + 1) * lanes)
-                        total = jnp.broadcast_to(taps[src, kw:kw + 1, lane], (tile, lanes))
-                        for b in range(8):
-                            slab = mix[s, pl.ds(base + b, tile + HALO), :]
-                            for a in range(HALO // 8 + 1):
-                                tap = 8 * a + b - lead
-                                if 0 <= tap < kw:
-                                    total = total + taps[src, tap:tap + 1, lane] * slab[8 * a:8 * a + tile]
-                        conv[src, pl.ds(base, tile), lane] = total
-
-            return carry
-
-        lax.fori_loop(0, 2, body, 0)
-
-    @pl.loop(1, nz)
-    def _(t):
-        each(t, relay(0))
-        each(t, relay(1))
-
-        @pl.when(t == nz - 1)
-        def _():
-            start_own(2)
-
-        each(t, diagonal(0))
-        compute(t - 1)
-        each(t, diagonal(1))
-        each(t, finish(0))
-        each(t, finish(1))
-
-    each(1, relay(2))
-    compute(nz - 1)
-
-    @pl.loop(2, nz - 1)
-    def _(t):
-        each(t, relay(2))
+                    lane = slice(s * lanes, (s + 1) * lanes)
+                    total = jnp.broadcast_to(taps[src, kw:kw + 1, lane], (tile, lanes))
+                    for b in range(8):
+                        slab = mix[side, s, pl.ds(base + b, tile + HALO), :]
+                        for a in range(HALO // 8 + 1):
+                            tap = 8 * a + b - lead
+                            if 0 <= tap < kw:
+                                total = total + taps[src, tap:tap + 1, lane] * slab[8 * a:8 * a + tile]
+                    conv[src, pl.ds(base, tile), lane] = total
+
+        on_planes(t, body)
+
+    slots = 2 * (nz - 1)
+
+    @pl.loop(0, slots)
+    def _(m):
+        each(1 + m // 2, relay(m % 2))
+
+        @pl.when((m % 2 == 1) & (1 + m // 2 == z) & has_up)
+        def _():
+            for i in range(2):
+                z_copy(2, z, i, True).start()
+
+        @pl.when((m % 2 == 1) & (1 + m // 2 == nz - 1 - z) & has_dn)
+        def _():
+            for i in range(2):
+                z_copy(2, z, i, False).start()
+
+        @pl.when(m >= 2)
+        def _():
+            each(m // 2, diagonal(m % 2))
+
+        @pl.when(m == 0)
+        def _():
+            gate(0)
+
+        @pl.when(m == 1)
+        def _():
+            convolve(0)
+
+    @pl.loop(0, slots)
+    def _(m):
+        t, i = 1 + m // 2, m % 2
+        each(t, onward(i))
+
+        @pl.when(m < 2)
+        def _():
+            each(nz - 1, diagonal(i))
+
+        @pl.when(m == 1)
+        def _():
+            each(1, sideways(0))
+            each(1, sideways(1))
+
+        @pl.when(m >= 2)
+        def _():
+            each(t, sideways(i))
+
+        @pl.when(i == 0)
+        def _():
+            @pl.when(m > 0)
+            def _():
+                convolve(t - 1)
+
+            each(t, finish(0))
+            each(t, finish(1))
+
+        @pl.when(i == 1)
+        def _():
+            gate(t)
+
+    convolve(nz - 1)
 
     channels = nz * block
 
@@ -278,24 +382,31 @@
             u = (v - mean) * scale * lng_ref[:, lane] + lnb_ref[:, lane]
             act[i, here, :] = (u * jax.nn.sigmoid(u)).astype(BF16)
 
-    if nz > 2:
-        each(nz - 1, relay(2))
-
-    @pl.loop(1, nz)
-    def _(t):
-        each(t, finish(2))
-
-    @pl.loop(0, nz)
-    def _(src):
-        d_copy(2, src, 1 - c).wait_recv()
+    def out_copy(n):
+        here = cols(p_cols(n), quarter)
+        return pltpu.make_async_copy(out_ref.at[:, here], out_any.at[:, here], out_sem.at[n])
 
     @pl.loop(0, 4)
     def _(n):
-        here = cols(n * quarter, quarter)
+        @pl.when(n == 2)
+        def _():
+            @pl.loop(1, nz)
+            def _(t):
+                each(t, arrived)
+
+        @pl.loop(0, nz)
+        def _(src):
+            p_copy(src, n, 1 - c).wait_recv()
+
+        here = cols(p_cols(n), quarter)
         total = x_ref[:, here].astype(F32)
         for i in range(nz):
             total = total + jnp.dot(act[i], held[2, i, :, here], preferred_element_type=F32)
         out_ref[:, here] = total.astype(BF16)
+        out_copy(n).start()
+
+    for n in range(4):
+        out_copy(n).wait()
 
     @pl.when(has_next)
     def _():
@@ -304,7 +415,11 @@
     for kind in range(3):
         @pl.loop(0, nz)
         def _(src):
-            d_copy(kind, src, c).wait_send()
+            if final(kind):
+                for slot in range(4):
+                    p_copy(src, slot, c).wait_send()
+            else:
+                d_copy(kind, src, c).wait_send()
 
             @pl.when(src != z)
             def _():
@@ -334,22 +449,24 @@
     out = pl.pallas_call(
         functools.partial(kernel, nsp, nz, kw),
         out_shape=jax.ShapeDtypeStruct((rows, width), BF16),
-        in_specs=[vmem, vmem, anyw, anyw, anyw, vmem, vmem, vmem, vmem],
-        out_specs=vmem,
+        in_specs=[anyw, vmem, anyw, anyw, anyw, vmem, vmem, vmem, vmem],
+        out_specs=anyw,
         scratch_shapes=[
+            pltpu.VMEM((rows, width), BF16),
+            pltpu.VMEM((rows, width), BF16),
             pltpu.VMEM((3, nz, block, width), BF16),
             pltpu.VMEM((HALO, width), BF16),
             pltpu.VMEM((HALO + rows, width), BF16),
-            pltpu.VMEM((block // lanes, HALO + rows + 8, lanes), F32),
+            pltpu.VMEM((2, block // lanes, HALO + rows + 8, lanes), F32),
             pltpu.VMEM((nz, rows, block), F32),
             pltpu.VMEM((nz, rows, block), BF16),
             pltpu.VMEM((nz, kw + 1, block), F32),
-            dma((3,)), dma((2,)),
+            dma((4,)), dma((4,)), dma((2,)),
             dma((3, nz, 2)), dma((3, nz, 2)), dma((3, nz, 2)), dma((3, nz)),
-            dma((3, nz, 2)), dma((3, nz, 2)), dma((3, nz, 2)), dma((3, nz, 2)), dma((3, nz)),
+            dma((3, nz, 2)), dma((3, nz, 2)), dma((3, nz, 2)), dma((3, nz, 2)), dma((3, nz)), dma((nz, 4)), dma((nz, 4)),
         ],
         compiler_params=pltpu.CompilerParams(
-            collective_id=0, has_side_effects=True, vmem_limit_bytes=56 * 1024 * 1024
+            collective_id=0, has_side_effects=True, vmem_limit_bytes=32 * 1024 * 1024
         ),
     )(
         stream[0], norm_gain[None], w_lin, w_gate, w_proj, conv_taps,

time: 71.6 us -> 66 us (0.922)
  Pallas kernels: 68.7 us -> 55.9 us
  local copies, waits for them, and re-layouts: 2.73 us -> 9.27 us
    pallas_call x1, Pallas kernels: 68.7 us -> 55.9 us  [local(): pl.pallas_call(functools.partial(kernel, nsp, nz, kw), out_shape=jax.Shap...]
    unnamed x1 -> x19, local copies, waits for them, and re-layouts: 2.73 us -> 9.27 us
where the time goes in v2:
time: 66 us; the launch traced here: 65.2 us
  Pallas kernels  55.9 us (85%)
  local copies, waits for them, and re-layouts  9.27 us (14%)
    pallas_call x1, Pallas kernels, local(): pl.pallas_call(functools.partial(kernel, nsp, nz, kw), out_shape=jax.Shap...  55.9 us
    unnamed x19, local copies, waits for them, and re-layouts  9.27 us

profile of v2, /device:TPU:1, one launch (start us, length us, event | category | flops | bytes accessed | tf_op | source)
XLA Modules:
  0.0 65.2 jit_solution(3377081290347382863)
XLA Ops:
  0.0 0.0 copy-start
  0.0 1.4 %copy-done = bf16[1,384,2048]{2,1,0:T(8,128)(2,1)S(1)} copy-done((bf16[1,384,2048]{2,1,0:T(8,128)(2,1)S(1)}, bf16[1,384,2048]{2,1,0:T(8,128)(2,1)}, u32[]{:S(2)}) %copy-start) | copy-done | bytes 1572888
  1.4 0.0 copy-start.1
  1.4 1.0 %copy-done.1 = bf16[128,2048]{1,0:T(8,128)(2,1)S(1)} copy-done((bf16[128,2048]{1,0:T(8,128)(2,1)S(1)}, bf16[128,2048]{1,0:T(8,128)(2,1)}, u32[]{:S(2)}) %copy-start.1) | copy-done | bytes 524312
  2.5 0.0 copy-start.2
  2.5 1.0 %copy-done.2 = bf16[128,2048]{1,0:T(8,128)(2,1)S(1)} copy-done((bf16[128,2048]{1,0:T(8,128)(2,1)S(1)}, bf16[128,2048]{1,0:T(8,128)(2,1)}, u32[]{:S(2)}) %copy-start.2) | copy-done | bytes 524312
  3.5 0.0 copy-start.3
  3.5 1.0 %copy-done.3 = bf16[128,2048]{1,0:T(8,128)(2,1)S(1)} copy-done((bf16[128,2048]{1,0:T(8,128)(2,1)S(1)}, bf16[128,2048]{1,0:T(8,128)(2,1)}, u32[]{:S(2)}) %copy-start.3) | copy-done | bytes 524312
  4.5 0.0 copy-start.4
  4.5 0.8 %copy-done.4 = bf16[31,1024]{1,0:T(8,128)(2,1)S(1)} copy-done((bf16[31,1024]{1,0:T(8,128)(2,1)S(1)}, bf16[31,1024]{1,0:T(8,128)(2,1)}, u32[]{:S(2)}) %copy-start.4) | copy-done | bytes 63512
  5.4 0.0 copy-start.5
  5.4 0.7 %copy-done.5 = f32[2048]{0:T(1024)S(1)} copy-done((f32[2048]{0:T(1024)S(1)}, f32[2048]{0:T(1024)}, u32[]{:S(2)}) %copy-start.5) | copy-done | bytes 8216
  6.1 0.0 copy-start.6
  6.1 0.7 %copy-done.6 = f32[1024]{0:T(1024)S(1)} copy-done((f32[1024]{0:T(1024)S(1)}, f32[1024]{0:T(1024)}, u32[]{:S(2)}) %copy-start.6) | copy-done | bytes 4120
  6.8 0.0 copy-start.7
  6.8 0.7 %copy-done.7 = f32[1024]{0:T(1024)S(1)} copy-done((f32[1024]{0:T(1024)S(1)}, f32[1024]{0:T(1024)}, u32[]{:S(2)}) %copy-start.7) | copy-done | bytes 4120
  7.4 0.0 copy-start.8
  7.4 0.7 %copy-done.8 = f32[1024]{0:T(1024)S(1)} copy-done((f32[1024]{0:T(1024)S(1)}, f32[1024]{0:T(1024)}, u32[]{:S(2)}) %copy-start.8) | copy-done | bytes 4120
  8.1 55.9 %shard_map.91 = bf16[384,2048]{1,0:T(8,128)(2,1)S(1)} custom-call(bf16[384,2048]{1,0:T(8,128)(2,1)S(1)} %bitcast.7, f32[1,2048]{1,0:T(1,128)S(1)} %bitcast.8, bf16[128,2048]{1,0:T(8,128)(2,1)S(1)} %copy-done.1, bf16[128,2048]{1,0:T(8,128)(2,1)S(1)} %copy-done.2, bf16[128,2048]{1,0:T(8,128)(2,1)S(1)} %copy-done.3, bf16[31,1024]{1,0:T(8,128)(2,1)S(1)} %copy-done.4, ...), custom_call_target="tpu_custom_call" | custom-call | tf_op jit(solution)/shard_map/pallas_call | solution.py:449
  64.1 1.1 %copy.11 = bf16[1,384,2048]{2,1,0:T(8,128)(2,1)} copy(bf16[1,384,2048]{2,1,0:T(8,128)(2,1)S(1)} %bitcast.6) | data formatting | bytes 3145728
Async XLA Ops:
  0.0 1.4 %copy-start = (bf16[1,384,2048]{2,1,0:T(8,128)(2,1)S(1)}, bf16[1,384,2048]{2,1,0:T(8,128)(2,1)}, u32[]{:S(2)}) copy-start(bf16[1,384,2048]{2,1,0:T(8,128)(2,1)} %param.9) | copy-start | bytes 4718596
  1.4 1.0 %copy-start.1 = (bf16[128,2048]{1,0:T(8,128)(2,1)S(1)}, bf16[128,2048]{1,0:T(8,128)(2,1)}, u32[]{:S(2)}) copy-start(bf16[128,2048]{1,0:T(8,128)(2,1)} %wl_ref.1) | copy-start | bytes 1572868
  2.5 1.0 %copy-start.2 = (bf16[128,2048]{1,0:T(8,128)(2,1)S(1)}, bf16[128,2048]{1,0:T(8,128)(2,1)}, u32[]{:S(2)}) copy-start(bf16[128,2048]{1,0:T(8,128)(2,1)} %wg_ref.1) | copy-start | bytes 1572868
  3.5 1.0 %copy-start.3 = (bf16[128,2048]{1,0:T(8,128)(2,1)S(1)}, bf16[128,2048]{1,0:T(8,128)(2,1)}, u32[]{:S(2)}) copy-start(bf16[128,2048]{1,0:T(8,128)(2,1)} %wp_ref.1) | copy-start | bytes 1572868
  4.5 0.8 %copy-start.4 = (bf16[31,1024]{1,0:T(8,128)(2,1)S(1)}, bf16[31,1024]{1,0:T(8,128)(2,1)}, u32[]{:S(2)}) copy-start(bf16[31,1024]{1,0:T(8,128)(2,1)} %taps_ref.1) | copy-start | bytes 190468
  5.4 0.7 %copy-start.5 = (f32[2048]{0:T(1024)S(1)}, f32[2048]{0:T(1024)}, u32[]{:S(2)}) copy-start(f32[2048]{0:T(1024)} %param.10) | copy-start | bytes 24580
  6.1 0.7 %copy-start.6 = (f32[1024]{0:T(1024)S(1)}, f32[1024]{0:T(1024)}, u32[]{:S(2)}) copy-start(f32[1024]{0:T(1024)} %param.14) | copy-start | bytes 12292
  6.8 0.7 %copy-start.7 = (f32[1024]{0:T(1024)S(1)}, f32[1024]{0:T(1024)}, u32[]{:S(2)}) copy-start(f32[1024]{0:T(1024)} %param.15) | copy-start | bytes 12292
  7.4 0.7 %copy-start.8 = (f32[1024]{0:T(1024)S(1)}, f32[1024]{0:T(1024)}, u32[]{:S(2)}) copy-start(f32[1024]{0:T(1024)} %param.16) | copy-start | bytes 12292

commit v3 on v2

--- a/solution.py
+++ b/solution.py
@@ -16,9 +16,9 @@
 
 def kernel(
     nsp, nz, kw,
-    x_any, gain_ref, wl_ref, wg_ref, wp_ref, taps_ref, bias_ref, lng_ref, lnb_ref,
+    x_any, gain_any, wl_ref, wg_ref, wp_ref, taps_any, bias_any, lng_any, lnb_any,
     out_any,
-    x_ref, out_ref, held, xh, normed, mix, conv, act, taps,
+    x_ref, out_ref, gain_ref, taps_ref, bias_ref, lng_ref, lnb_ref, held, xh, normed, mix, conv, act, taps,
     local_sem, out_sem, halo_sem, z_recv, x_recv, y_recv, d_recv, up_send, dn_send, x_send, y_send, d_send, dp_recv, dp_send,
 ):
     rows, width = x_ref.shape
@@ -114,6 +114,14 @@
     mine[0].start()
     stream_in.start()
     mine[1].start()
+    small = [
+        pltpu.make_async_copy(ref, there, local_sem.at[4 + i])
+        for i, (ref, there) in enumerate((
+            (gain_any, gain_ref), (taps_any, taps_ref), (bias_any, bias_ref), (lng_any, lng_ref), (lnb_any, lnb_ref),
+        ))
+    ]
+    for copy in small:
+        copy.start()
     mine[2].start()
 
     barrier = pltpu.get_barrier_semaphore()
@@ -245,6 +253,8 @@
             scale = lax.rsqrt(jnp.mean(full * full, axis=1, keepdims=True) + EPS)
             normed[pl.ds(pl.multiple_of(base + r * 16, 16), 16), :] = (full * scale * gain_ref[...]).astype(BF16)
 
+    for copy in small:
+        copy.wait()
     norm_into(x_ref, HALO, rows)
     for i in range(nz):
         taps[i, 0:kw] = taps_ref[:, i * block:(i + 1) * block].astype(F32)
@@ -443,17 +453,21 @@
     nz = ntp // 2
     block = channels // nz
     lanes = min(128, block)
-    vmem = pl.BlockSpec(memory_space=pltpu.VMEM)
-    anyw = pl.BlockSpec(memory_space=pl.ANY)
+    kept = pl.BlockSpec(memory_space=pltpu.HBM)
     dma = pltpu.SemaphoreType.DMA
     out = pl.pallas_call(
         functools.partial(kernel, nsp, nz, kw),
         out_shape=jax.ShapeDtypeStruct((rows, width), BF16),
-        in_specs=[anyw, vmem, anyw, anyw, anyw, vmem, vmem, vmem, vmem],
-        out_specs=anyw,
+        in_specs=[kept] * 9,
+        out_specs=pl.BlockSpec(memory_space=pl.ANY),
         scratch_shapes=[
             pltpu.VMEM((rows, width), BF16),
             pltpu.VMEM((rows, width), BF16),
+            pltpu.VMEM((1, width), F32),
+            pltpu.VMEM((kw, channels), BF16),
+            pltpu.VMEM((1, channels), F32),
+            pltpu.VMEM((1, channels), F32),
+            pltpu.VMEM((1, channels), F32),
             pltpu.VMEM((3, nz, block, width), BF16),
             pltpu.VMEM((HALO, width), BF16),
             pltpu.VMEM((HALO + rows, width), BF16),
@@ -461,12 +475,12 @@
             pltpu.VMEM((nz, rows, block), F32),
             pltpu.VMEM((nz, rows, block), BF16),
             pltpu.VMEM((nz, kw + 1, block), F32),
-            dma((4,)), dma((4,)), dma((2,)),
+            dma((9,)), dma((4,)), dma((2,)),
             dma((3, nz, 2)), dma((3, nz, 2)), dma((3, nz, 2)), dma((3, nz)),
             dma((3, nz, 2)), dma((3, nz, 2)), dma((3, nz, 2)), dma((3, nz, 2)), dma((3, nz)), dma((nz, 4)), dma((nz, 4)),
         ],
         compiler_params=pltpu.CompilerParams(
-            collective_id=0, has_side_effects=True, vmem_limit_bytes=32 * 1024 * 1024
+            collective_id=0, has_side_effects=True, vmem_limit_bytes=60 * 1024 * 1024
         ),
     )(
         stream[0], norm_gain[None], w_lin, w_gate, w_proj, conv_taps,

time: 66 us -> 59.9 us (0.908)
  local copies, waits for them, and re-layouts: 9.27 us -> 2.73 us
  Pallas kernels: 55.9 us -> 56.7 us
    unnamed x19 -> x1, local copies, waits for them, and re-layouts: 9.27 us -> 2.73 us
    pallas_call x1, Pallas kernels: 55.9 us -> 56.7 us  [local(): pl.pallas_call(functools.partial(kernel, nsp, nz, kw), out_shape=jax.Shap...]
where the time goes in v3:
time: 59.9 us; the launch traced here: 59.4 us
  Pallas kernels  56.7 us (95%)
  local copies, waits for them, and re-layouts  2.73 us (5%)
    pallas_call x1, Pallas kernels, local(): pl.pallas_call(functools.partial(kernel, nsp, nz, kw), out_shape=jax.Shap...  56.7 us
    unnamed x1, local copies, waits for them, and re-layouts  2.73 us

profile of v3, /device:TPU:1, one launch (start us, length us, event | category | flops | bytes accessed | tf_op | source)
XLA Modules:
  0.0 59.4 jit_solution(10255006705198978347)
XLA Ops:
  0.0 56.7 %shard_map.91 = bf16[384,2048]{1,0:T(8,128)(2,1)} custom-call(bf16[384,2048]{1,0:T(8,128)(2,1)} %bitcast.7, f32[1,2048]{1,0:T(1,128)} %bitcast.8, bf16[128,2048]{1,0:T(8,128)(2,1)} %wl_ref.1, bf16[128,2048]{1,0:T(8,128)(2,1)} %wg_ref.1, bf16[128,2048]{1,0:T(8,128)(2,1)} %wp_ref.1, bf16[31,1024]{1,0:T(8,128)(2,1)} %taps_any.1, f32[1,1024]{1,0:T(1,128)} %bitcast.9, ...), custom_call_target="tpu_custom_call" | custom-call | tf_op jit(solution)/shard_map/pallas_call | solution.py:458
  56.7 2.7 %copy.11 = bf16[1,384,2048]{2,1,0:T(8,128)(2,1)} copy(bf16[1,384,2048]{2,1,0:T(8,128)(2,1)} %bitcast.6) | data formatting | bytes 3145728
